TPU v7x, 32 devices: a whole 2x2x4 slice. The times are simulated.
32 devices in a mesh: grp: 2 (over y), sp: 4 (over z), tp: 4 (over x, core).
Axes of the slice: x: 2, y: 2, z: 4, core: 2. Of those that a mesh axis runs over, the one named last changes fastest.
Arguments:
- tokens: bfloat16 [3072, 4096], P(('grp', 'sp'), 'tp'), parts along dimension 0, may hold values from -6 to 6
- proj_b: bfloat16 [2, 4096, 2048], P(None, 'sp', 'tp'), may hold values from -0.09375 to 0.09375
- proj_c: bfloat16 [2, 4096, 2048], P(None, 'sp', 'tp'), may hold values from -0.09375 to 0.09375
- proj_x: bfloat16 [2, 4096, 2048], P(None, 'sp', 'tp'), may hold values from -0.09375 to 0.09375
- proj_out: bfloat16 [2, 2048, 4096], P(None, 'sp', 'tp'), may hold values from -1 to 1
- conv_taps: float32 [2, 3, 2048], P(None, None, 'tp'), may hold values from -3 to 3
- ln_gain: float32 [2, 4096], P(None, 'tp'), may hold values from 0.1 to 1.9
- ln_bias: float32 [2, 4096], P(None, 'tp'), may hold values from -2 to 2
Outputs:
- result: bfloat16 [3072, 4096], P(('grp', 'sp'), 'tp'), parts along dimension 0
There are 2 independent parts, one for each index of `grp`. A program takes and returns all parts, laid end to end along the dimension named above; an argument that names none is the same for every part. Nothing has to cross between parts.
All inputs are finite; a program needn't handle non-finite values.
Results may differ from a plain program's by a relative error of at most 0.012.
Values may be sent and summed in bfloat16 or wider, within the bound.
A program may use at most 128 MiB of HBM per device.

v0:
```python
import jax
import jax.numpy as jnp
from jax import lax
from jax.sharding import PartitionSpec as P

LAYERS = 2
norm_eps = 1e-05


def from_behind(block, axis, distance):
    devices = range(lax.axis_size(axis))
    route = [(i - distance, i) for i in devices if i - distance in devices]
    return lax.ppermute(block, axis, route)


def local(tokens, proj_b, proj_c, proj_x, proj_out, conv_taps, ln_gain, ln_bias):
    residual_scale = (2.0 * LAYERS) ** 0.25
    hidden = tokens
    whole_b, whole_c, whole_x, whole_out = (
        lax.all_gather(proj_b, "sp", axis=1, tiled=True),
        lax.all_gather(proj_c, "sp", axis=1, tiled=True),
        lax.all_gather(proj_x, "sp", axis=1, tiled=True),
        lax.all_gather(proj_out, "sp", axis=1, tiled=True),
    )
    for layer_index in range(LAYERS):
        gathered = lax.all_gather(hidden, "tp", axis=1, tiled=True)
        count_rows = gathered.shape[0]
        acc_b = jnp.dot(gathered, whole_b[layer_index], preferred_element_type=jnp.float32)
        acc_c = jnp.dot(gathered, whole_c[layer_index], preferred_element_type=jnp.float32)
        acc_x = jnp.dot(gathered, whole_x[layer_index], preferred_element_type=jnp.float32)
        out_gate = lax.optimization_barrier(acc_b.astype(jnp.bfloat16))
        in_gate = lax.optimization_barrier(acc_c.astype(jnp.bfloat16))
        values = lax.optimization_barrier(acc_x.astype(jnp.bfloat16))
        gated_in = in_gate.astype(jnp.float32) * values.astype(jnp.float32)
        reach = conv_taps.shape[1] - 1
        fringe = from_behind(gated_in[count_rows - reach :], "sp", 1)
        padded = jnp.concatenate([fringe, gated_in], 0)
        conv_out = jnp.zeros_like(gated_in)
        for tap_index in range(reach + 1):
            conv_out = (
                conv_out
                + conv_taps[layer_index, tap_index] * padded[tap_index : tap_index + count_rows]
            )
        branch = (out_gate.astype(jnp.float32) * conv_out).astype(jnp.bfloat16)
        all_branch = lax.all_gather(branch, "tp", axis=1, tiled=True)
        acc_out = jnp.dot(all_branch, whole_out[layer_index], preferred_element_type=jnp.float32)
        mixed = lax.optimization_barrier(acc_out.astype(jnp.bfloat16))
        summed = residual_scale * hidden.astype(jnp.float32) + mixed.astype(jnp.float32)
        width_all = summed.shape[1] * lax.axis_size("tp")
        mean = (lax.psum(jnp.sum(summed, axis=1), "tp") / width_all)[:, None]
        centered = summed - mean
        variance = (lax.psum(jnp.sum(centered * centered, axis=1), "tp") / width_all)[:, None]
        hidden = (
            centered * lax.rsqrt(variance + norm_eps) * ln_gain[layer_index] + ln_bias[layer_index]
        ).astype(jnp.bfloat16)
    return hidden


def solution(mesh):
    return jax.shard_map(
        local,
        mesh=mesh,
        in_specs=(
            P(("grp", "sp"), "tp"),
            P(None, "sp", "tp"),
            P(None, "sp", "tp"),
            P(None, "sp", "tp"),
            P(None, "sp", "tp"),
            P(None, None, "tp"),
            P(None, "tp"),
            P(None, "tp"),
        ),
        out_specs=P(("grp", "sp"), "tp"),
        check_vma=False,
    )
```

profile of v0, /device:TPU:0, one launch (start us, length us, event | category | flops | bytes accessed | tf_op | source)
XLA Modules:
  0.0 767.4 jit_solution(15799623841625418125)
XLA Ops:
  6.5 0.7 all-gather.9.cloned.1.call-update
  7.3 0.0 all-gather.13.cloned.1.call-start
  7.3 0.7 all-gather.13.cloned.1.call-update
  8.0 0.0 all-gather.15.cloned.1.call-start
  8.1 0.7 all-gather.15.cloned.1.call-update
  8.8 0.0 all-gather.11.cloned.1.call-start
  8.8 0.5 all-gather.11.cloned.1.call-update
  9.3 0.0 all-gather.19.cloned.1.call-start
  9.4 0.5 all-gather.19.cloned.1.call-update
  9.9 0.0 all-gather.17.cloned.1.call-start
  10.0 30.2 %all-gather.9.cloned.1.call-done = bf16[384,4096]{1,0:T(8,128)(2,1)} async-done(((bf16[384,1024]{1,0:T(8,128)(2,1)}), bf16[384,4096]{1,0:T(8,128)(2,1)}) %all-gather.9.cloned.1.call-update) | async-done | bytes 3145744 | tf_op jit(solution)/shard_map/all_gather | solution.py:26
  40.2 151.2 %all-gather.13.cloned.1.call-done = bf16[2,4096,512]{2,1,0:T(8,128)(2,1)} async-done(((bf16[2,1024,512]{2,1,0:T(8,128)(2,1)}), bf16[2,4096,512]{2,1,0:T(8,128)(2,1)}) %all-gather.13.cloned.1.call-update) | async-done | bytes 8388624 | tf_op jit(solution)/shard_map/all_gather | solution.py:21
  191.4 4.9 fusion.11
  196.3 144.5 %all-gather.15.cloned.1.call-done = bf16[2,4096,512]{2,1,0:T(8,128)(2,1)} async-done(((bf16[2,1024,512]{2,1,0:T(8,128)(2,1)}), bf16[2,4096,512]{2,1,0:T(8,128)(2,1)}) %all-gather.15.cloned.1.call-update) | async-done | bytes 8388624 | tf_op jit(solution)/shard_map/all_gather | solution.py:22
  340.8 4.9 fusion.12
  345.7 0.1 convert_multiply_fusion.1
  345.8 1.3 collective-permute-start
  347.1 142.9 %all-gather.11.cloned.1.call-done = bf16[2,4096,512]{2,1,0:T(8,128)(2,1)} async-done(((bf16[2,1024,512]{2,1,0:T(8,128)(2,1)}), bf16[2,4096,512]{2,1,0:T(8,128)(2,1)}) %all-gather.11.cloned.1.call-update) | async-done | bytes 8388624 | tf_op jit(solution)/shard_map/all_gather | solution.py:20
  490.0 4.9 fusion.10
  495.0 0.0 copy-start.4
  495.0 1.1 fusion.29
  496.1 0.0 all-gather.17.cloned.1.call-update
  496.1 0.0 all-gather.21.cloned.1.call-start
  496.2 143.1 %all-gather.19.cloned.1.call-done = bf16[2,2048,1024]{2,1,0:T(8,128)(2,1)} async-done(((bf16[2,512,1024]{2,1,0:T(8,128)(2,1)}), bf16[2,2048,1024]{2,1,0:T(8,128)(2,1)}) %all-gather.19.cloned.1.call-update) | async-done | bytes 8388624 | tf_op jit(solution)/shard_map/all_gather | solution.py:23
  639.3 19.3 %all-gather.17.cloned.1.call-done = bf16[384,2048]{1,0:T(8,128)(2,1)} async-done(((bf16[384,512]{1,0:T(8,128)(2,1)}), bf16[384,2048]{1,0:T(8,128)(2,1)}) %all-gather.17.cloned.1.call-update) | async-done | bytes 1572880 | tf_op jit(solution)/shard_map/all_gather | solution.py:45
  658.6 4.5 fusion.8
  663.0 0.3 fusion.16
  663.4 5.9 psum.28
  669.2 0.4 multiply_reduce_fusion.1
  669.7 5.7 psum.29
  675.3 1.3 add_convert_fusion.1
  676.7 0.0 all-gather.21.cloned.1.call-update
  676.7 0.0 all-gather.23.cloned.1.call-start
  676.8 29.9 %all-gather.21.cloned.1.call-done = bf16[384,4096]{1,0:T(8,128)(2,1)} async-done(((bf16[384,1024]{1,0:T(8,128)(2,1)}), bf16[384,4096]{1,0:T(8,128)(2,1)}) %all-gather.21.cloned.1.call-update) | async-done | bytes 3145744 | tf_op jit(solution)/shard_map/all_gather | solution.py:26
  706.7 5.1 fusion.14
  711.8 4.1 fusion.15
  715.9 0.1 convert_multiply_fusion
  716.0 3.6 collective-permute-start.1
  719.6 1.8 fusion.13
  721.4 1.0 fusion.23
  722.5 0.0 all-gather.23.cloned.1.call-update
  722.5 19.9 %all-gather.23.cloned.1.call-done = bf16[384,2048]{1,0:T(8,128)(2,1)} async-done(((bf16[384,512]{1,0:T(8,128)(2,1)}), bf16[384,2048]{1,0:T(8,128)(2,1)}) %all-gather.23.cloned.1.call-update) | async-done | bytes 1572880 | tf_op jit(solution)/shard_map/all_gather | solution.py:45
  742.4 4.5 fusion.9
  746.9 0.3 fusion.17
  747.2 5.9 psum.30
  753.1 0.4 multiply_reduce_fusion
  753.5 5.7 psum.31
  759.2 1.3 add_convert_fusion
  (28 shorter events, 0.1 us)
Async XLA Ops:
  6.5 33.6 %all-gather.9.cloned.1.call-start = ((), (), s32[]{:S(2)}) async-start(), calls=%async_computation | async-start | bytes 3932160 | tf_op jit(solution)/shard_map/all_gather | solution.py:26
  7.3 184.1 %all-gather.13.cloned.1.call-start = ((), (), s32[]{:S(2)}) async-start(), calls=%async_computation.2 | async-start | bytes 10485760 | tf_op jit(solution)/shard_map/all_gather | solution.py:21
  8.0 332.8 %all-gather.15.cloned.1.call-start = ((), (), s32[]{:S(2)}) async-start(), calls=%async_computation.3 | async-start | bytes 10485760 | tf_op jit(solution)/shard_map/all_gather | solution.py:22
  8.7 1.2 copy-start.2
  8.8 481.3 %all-gather.11.cloned.1.call-start = ((), (), s32[]{:S(2)}) async-start(), calls=%async_computation.1 | async-start | bytes 10485760 | tf_op jit(solution)/shard_map/all_gather | solution.py:20
  9.3 630.0 %all-gather.19.cloned.1.call-start = ((), (), s32[]{:S(2)}) async-start(), calls=%async_computation.5 | async-start | bytes 10485760 | tf_op jit(solution)/shard_map/all_gather | solution.py:23
  9.9 648.6 %all-gather.17.cloned.1.call-start = ((), (), s32[]{:S(2)}) async-start(), calls=%async_computation.4 | async-start | bytes 1966080 | tf_op jit(solution)/shard_map/all_gather | solution.py:45
  345.8 149.2 %collective-permute-start = (f32[2,512]{1,0:T(2,128)S(1)}, f32[2,512]{1,0:T(2,128)S(1)}, u32[]{:S(2)}, u32[]{:S(2)}) collective-permute-start(f32[2,512]{1,0:T(2,128)S(1)} %slice.99), channel_id=1, source_target_pairs={{0,4},{4,8},{8,12},{1,5},{5,9},{9,13},{2,6},{6,10},{10,14},{3,7},{... | collective-permute-start | bytes 12296 | tf_op jit(solution)/shard_map/ppermute | solution.py:13
  495.0 1.2 copy-start.3
  495.0 1.2 copy-start.4
  496.1 210.6 %all-gather.21.cloned.1.call-start = ((), (), s32[]{:S(2)}) async-start(), calls=%async_computation.6 | async-start | bytes 3932160 | tf_op jit(solution)/shard_map/all_gather | solution.py:26
  496.2 166.8 %copy-start.1 = (bf16[384,1024]{1,0:T(8,128)(2,1)S(1)}, bf16[384,1024]{1,0:T(8,128)(2,1)}, u32[]{:S(2)}) copy-start(bf16[384,1024]{1,0:T(8,128)(2,1)} %param.8) | copy-start | bytes 2359300
  676.7 65.7 %all-gather.23.cloned.1.call-start = ((), (), s32[]{:S(2)}) async-start(), calls=%async_computation.7 | async-start | bytes 1966080 | tf_op jit(solution)/shard_map/all_gather | solution.py:45
  706.7 5.1 copy-start.5
  706.7 12.9 %slice-start = ((s8[8388608]{0:T(1024)(128)(4,1)}), s8[4194304]{0:T(1024)(128)(4,1)S(1)}, s32[]{:S(2)}) async-start(s8[8388608]{0:T(1024)(128)(4,1)} %bitcast.68), calls=%async_computation.8 | async-start | bytes 8388608
  711.8 7.9 %slice-start.1 = ((s8[8388608]{0:T(1024)(128)(4,1)}), s8[4194304]{0:T(1024)(128)(4,1)S(1)}, s32[]{:S(2)}) async-start(s8[8388608]{0:T(1024)(128)(4,1)} %bitcast.68), calls=%async_computation.9 | async-start | bytes 8388608
  716.0 5.4 collective-permute-start.1
  722.5 24.3 %copy-start = (bf16[384,1024]{1,0:T(8,128)(2,1)S(1)}, bf16[384,1024]{1,0:T(8,128)(2,1)}, u32[]{:S(2)}) copy-start(bf16[384,1024]{1,0:T(8,128)(2,1)} %add_convert_fusion.1) | copy-start | bytes 2359300
Sparse Core Ops, SparseCore 0:
  8.9 31.2 all-gather.8
  41.7 149.6 all-gather.12
  192.9 147.7 all-gather.14
  342.2 147.7 all-gather.10
  491.5 147.7 all-gather.18
  640.7 17.8 all-gather.16
  676.8 29.8 all-gather.20
  722.6 19.7 all-gather.22
where the time goes:
time: 768 us; the launch traced here: 767 us
  waiting for transfers between devices  684 us (89%)
  matrix products  34.6 us (5%)
  blocking collectives  23.1 us (3%)
  between operations  13.8 us (2%)
    all_gather x1, waiting for transfers between devices, local(): lax.all_gather(proj_c, 'sp', axis=1, tiled=True)  151 us
    all_gather x1, waiting for transfers between devices, local(): lax.all_gather(proj_x, 'sp', axis=1, tiled=True)  144 us
    all_gather x1, waiting for transfers between devices, local(): lax.all_gather(proj_out, 'sp', axis=1, tiled=True)  143 us
    all_gather x1, waiting for transfers between devices, local(): lax.all_gather(proj_b, 'sp', axis=1, tiled=True)  143 us
    all_gather x2, waiting for transfers between devices, local(): gathered = lax.all_gather(hidden, 'tp', axis=1, tiled=True)  60.1 us
    all_gather x2, waiting for transfers between devices, local(): all_branch = lax.all_gather(branch, 'tp', axis=1, tiled=True)  39.1 us
  transfers between devices with their start and end apart: 10, of which 8 were waited for; matrix products, arithmetic and copies ran while one was open for 2% of the time, Pallas kernels for 0%

commit v1 on v0

--- a/solution.py
+++ b/solution.py
@@ -42,7 +42,14 @@
                 + conv_taps[layer_index, tap_index] * padded[tap_index : tap_index + count_rows]
             )
         branch = (out_gate.astype(jnp.float32) * conv_out).astype(jnp.bfloat16)
-        all_branch = lax.all_gather(branch, "tp", axis=1, tiled=True)
+        ring = [branch]
+        for hop in range(3):
+            ring.append(lax.ppermute(ring[-1], "tp", [(dev, (dev + 1) % 4) for dev in range(4)]))
+        all_branch = jnp.roll(
+            jnp.concatenate(ring[::-1], axis=1),
+            (lax.axis_index("tp") + 1) * ring[0].shape[1],
+            axis=1,
+        )
         acc_out = jnp.dot(all_branch, whole_out[layer_index], preferred_element_type=jnp.float32)
         mixed = lax.optimization_barrier(acc_out.astype(jnp.bfloat16))
         summed = residual_scale * hidden.astype(jnp.float32) + mixed.astype(jnp.float32)

time: 768 us -> 747 us (0.973)
  waiting for transfers between devices: 684 us -> 663 us
    all_gather x2 -> x0, waiting for transfers between devices: 39.1 us -> none  [local(): all_branch = lax.all_gather(branch, 'tp', axis=1, tiled=True)]
    ppermute x0 -> x6, waiting for transfers between devices: none -> 36 us  [local(): lax.ppermute(ring[-1], 'tp', [(dev, (dev + 1) % 4) for dev in range(4)])]
    all_gather x1, waiting for transfers between devices: 143 us -> 129 us  [local(): lax.all_gather(proj_out, 'sp', axis=1, tiled=True)]
  transfers between devices with their start and end apart: 10 -> 14, of which waited for: 8 -> 11; matrix products, arithmetic and copies ran while one was open for 2% -> 2% of each run, Pallas kernels for 0% -> 0%
where the time goes in v1:
time: 747 us; the launch traced here: 746 us
  waiting for transfers between devices  663 us (89%)
  matrix products  34.3 us (5%)
  blocking collectives  24.5 us (3%)
  between operations  13.8 us (2%)
    all_gather x1, waiting for transfers between devices, local(): lax.all_gather(proj_c, 'sp', axis=1, tiled=True)  151 us
    all_gather x1, waiting for transfers between devices, local(): lax.all_gather(proj_x, 'sp', axis=1, tiled=True)  144 us
    all_gather x1, waiting for transfers between devices, local(): lax.all_gather(proj_b, 'sp', axis=1, tiled=True)  143 us
    all_gather x1, waiting for transfers between devices, local(): lax.all_gather(proj_out, 'sp', axis=1, tiled=True)  129 us
    all_gather x2, waiting for transfers between devices, local(): gathered = lax.all_gather(hidden, 'tp', axis=1, tiled=True)  56.1 us
    ppermute x6, waiting for transfers between devices, local(): lax.ppermute(ring[-1], 'tp', [(dev, (dev + 1) % 4) for dev in range(4)])  36 us
  transfers between devices with their start and end apart: 14, of which 11 were waited for; matrix products, arithmetic and copies ran while one was open for 2% of the time, Pallas kernels for 0%

profile of v1, /device:TPU:0, one launch (start us, length us, event | category | flops | bytes accessed | tf_op | source)
XLA Modules:
  0.0 746.4 jit_solution(8761755600681385672)
XLA Ops:
  6.5 0.7 all-gather.7.cloned.1.call-update
  7.3 0.0 all-gather.11.cloned.1.call-start
  7.3 0.7 all-gather.11.cloned.1.call-update
  8.0 0.0 all-gather.13.cloned.1.call-start
  8.1 0.7 all-gather.13.cloned.1.call-update
  8.8 0.0 all-gather.9.cloned.1.call-start
  8.8 0.5 all-gather.9.cloned.1.call-update
  9.3 0.0 all-gather.15.cloned.1.call-start
  9.4 0.5 all-gather.15.cloned.1.call-update
  9.9 0.0 all-gather.17.cloned.1.call-start
  10.0 30.2 %all-gather.7.cloned.1.call-done = bf16[384,4096]{1,0:T(8,128)(2,1)} async-done(((bf16[384,1024]{1,0:T(8,128)(2,1)}), bf16[384,4096]{1,0:T(8,128)(2,1)}) %all-gather.7.cloned.1.call-update) | async-done | bytes 3145744 | tf_op jit(solution)/shard_map/all_gather | solution.py:26
  40.2 151.2 %all-gather.11.cloned.1.call-done = bf16[2,4096,512]{2,1,0:T(8,128)(2,1)} async-done(((bf16[2,1024,512]{2,1,0:T(8,128)(2,1)}), bf16[2,4096,512]{2,1,0:T(8,128)(2,1)}) %all-gather.11.cloned.1.call-update) | async-done | bytes 8388624 | tf_op jit(solution)/shard_map/all_gather | solution.py:21
  191.4 4.9 fusion.33
  196.3 144.5 %all-gather.13.cloned.1.call-done = bf16[2,4096,512]{2,1,0:T(8,128)(2,1)} async-done(((bf16[2,1024,512]{2,1,0:T(8,128)(2,1)}), bf16[2,4096,512]{2,1,0:T(8,128)(2,1)}) %all-gather.13.cloned.1.call-update) | async-done | bytes 8388624 | tf_op jit(solution)/shard_map/all_gather | solution.py:22
  340.8 4.9 fusion.34
  345.7 0.1 convert_multiply_fusion.1
  345.9 1.4 collective-permute-start
  347.3 142.7 %all-gather.9.cloned.1.call-done = bf16[2,4096,512]{2,1,0:T(8,128)(2,1)} async-done(((bf16[2,1024,512]{2,1,0:T(8,128)(2,1)}), bf16[2,4096,512]{2,1,0:T(8,128)(2,1)}) %all-gather.9.cloned.1.call-update) | async-done | bytes 8388624 | tf_op jit(solution)/shard_map/all_gather | solution.py:20
  490.0 4.9 fusion.32
  495.0 0.3 fusion.51
  495.3 0.1 collective-permute-start.1
  495.4 7.2 collective-permute-done.1
  502.5 7.2 collective-permute-done.2
  509.8 129.5 %all-gather.15.cloned.1.call-done = bf16[2,2048,1024]{2,1,0:T(8,128)(2,1)} async-done(((bf16[2,512,1024]{2,1,0:T(8,128)(2,1)}), bf16[2,2048,1024]{2,1,0:T(8,128)(2,1)}) %all-gather.15.cloned.1.call-update) | async-done | bytes 8388624 | tf_op jit(solution)/shard_map/all_gather | solution.py:23
  639.3 5.3 fusion.26
  644.6 0.3 fusion.38
  644.9 6.8 psum.28
  651.8 0.4 multiply_reduce_fusion.1
  652.2 5.9 psum.29
  658.2 1.3 add_convert_fusion.1
  659.5 0.0 all-gather.17.cloned.1.call-update
  659.5 25.9 %all-gather.17.cloned.1.call-done = bf16[384,4096]{1,0:T(8,128)(2,1)} async-done(((bf16[384,1024]{1,0:T(8,128)(2,1)}), bf16[384,4096]{1,0:T(8,128)(2,1)}) %all-gather.17.cloned.1.call-update) | async-done | bytes 3145744 | tf_op jit(solution)/shard_map/all_gather | solution.py:26
  685.4 5.1 fusion.36
  690.5 4.2 fusion.37
  694.7 0.1 convert_multiply_fusion
  694.8 3.8 collective-permute-start.4
  698.7 1.8 fusion.35
  700.5 0.3 fusion.45
  700.8 0.1 collective-permute-start.5
  700.9 7.2 collective-permute-done.5
  708.1 7.2 collective-permute-done.6
  715.3 7.2 collective-permute-done.7
  722.5 3.2 fusion.29
  725.7 0.3 fusion.39
  726.0 6.0 psum.30
  732.0 0.4 multiply_reduce_fusion
  732.4 5.8 psum.31
  738.2 1.3 add_convert_fusion
  (39 shorter events, 0.1 us)
Async XLA Ops:
  6.5 33.6 %all-gather.7.cloned.1.call-start = ((), (), s32[]{:S(2)}) async-start(), calls=%async_computation | async-start | bytes 3932160 | tf_op jit(solution)/shard_map/all_gather | solution.py:26
  7.3 184.1 %all-gather.11.cloned.1.call-start = ((), (), s32[]{:S(2)}) async-start(), calls=%async_computation.2 | async-start | bytes 10485760 | tf_op jit(solution)/shard_map/all_gather | solution.py:21
  8.0 2.0 copy-start.2
  8.0 332.8 %all-gather.13.cloned.1.call-start = ((), (), s32[]{:S(2)}) async-start(), calls=%async_computation.3 | async-start | bytes 10485760 | tf_op jit(solution)/shard_map/all_gather | solution.py:22
  8.8 481.3 %all-gather.9.cloned.1.call-start = ((), (), s32[]{:S(2)}) async-start(), calls=%async_computation.1 | async-start | bytes 10485760 | tf_op jit(solution)/shard_map/all_gather | solution.py:20
  9.3 630.0 %all-gather.15.cloned.1.call-start = ((), (), s32[]{:S(2)}) async-start(), calls=%async_computation.4 | async-start | bytes 10485760 | tf_op jit(solution)/shard_map/all_gather | solution.py:23
  9.9 675.5 %all-gather.17.cloned.1.call-start = ((), (), s32[]{:S(2)}) async-start(), calls=%async_computation.5 | async-start | bytes 3932160 | tf_op jit(solution)/shard_map/all_gather | solution.py:26
  345.8 163.9 %copy-start.3 = (f32[2,1024]{1,0:T(2,128)S(1)}, f32[2,1024]{1,0:T(2,128)}, u32[]{:S(2)}) copy-start(f32[2,1024]{1,0:T(2,128)} %param.16) | copy-start | bytes 24580
  345.8 163.9 %copy-start.4 = (f32[2,1024]{1,0:T(2,128)S(1)}, f32[2,1024]{1,0:T(2,128)}, u32[]{:S(2)}) copy-start(f32[2,1024]{1,0:T(2,128)} %param.17) | copy-start | bytes 24580
  345.9 149.1 %collective-permute-start = (f32[2,512]{1,0:T(2,128)S(1)}, f32[2,512]{1,0:T(2,128)S(1)}, u32[]{:S(2)}, u32[]{:S(2)}) collective-permute-start(f32[2,512]{1,0:T(2,128)S(1)} %slice.99), channel_id=1, source_target_pairs={{0,4},{4,8},{8,12},{1,5},{5,9},{9,13},{2,6},{6,10},{10,14},{3,7},{... | collective-permute-start | bytes 12296 | tf_op jit(solution)/shard_map/ppermute | solution.py:13
  495.3 7.3 collective-permute-start.1
  502.5 7.2 collective-permute-start.2
  509.7 129.5 %collective-permute-start.3 = (bf16[384,512]{1,0:T(8,128)(2,1)S(1)}, bf16[384,512]{1,0:T(8,128)(2,1)S(1)}, u32[]{:S(2)}, u32[]{:S(2)}) collective-permute-start(bf16[384,512]{1,0:T(8,128)(2,1)S(1)} %collective-permute-done.2), channel_id=1, source_target_pairs={{0,1},{1,2},{2,3},{3,0},{4,5},{5,6},{6,7},{7,4},{8,9},{9,10},{10,1... | collective-permute-start | bytes 1179656 | tf_op jit(solution)/shard_map/ppermute | solution.py:47
  509.8 134.8 %copy-start.1 = (bf16[384,1024]{1,0:T(8,128)(2,1)S(1)}, bf16[384,1024]{1,0:T(8,128)(2,1)}, u32[]{:S(2)}) copy-start(bf16[384,1024]{1,0:T(8,128)(2,1)} %param.10) | copy-start | bytes 2359300
  685.4 5.1 copy-start.5
  685.4 13.3 %slice-start.2 = ((s8[8388608]{0:T(1024)(128)(4,1)}), s8[4194304]{0:T(1024)(128)(4,1)S(1)}, s32[]{:S(2)}) async-start(s8[8388608]{0:T(1024)(128)(4,1)} %bitcast.68), calls=%async_computation.8 | async-start | bytes 8388608
  690.5 8.2 %slice-start.3 = ((s8[8388608]{0:T(1024)(128)(4,1)}), s8[4194304]{0:T(1024)(128)(4,1)S(1)}, s32[]{:S(2)}) async-start(s8[8388608]{0:T(1024)(128)(4,1)} %bitcast.68), calls=%async_computation.9 | async-start | bytes 8388608
  694.7 27.8 %slice-start = ((s8[8388608]{0:T(1024)(128)(4,1)}), s8[4194304]{0:T(1024)(128)(4,1)S(1)}, s32[]{:S(2)}) async-start(s8[8388608]{0:T(1024)(128)(4,1)} %bitcast.66), calls=%async_computation.6 | async-start | bytes 8388608
  694.8 27.7 %slice-start.1 = ((s8[8388608]{0:T(1024)(128)(4,1)}), s8[4194304]{0:T(1024)(128)(4,1)S(1)}, s32[]{:S(2)}) async-start(s8[8388608]{0:T(1024)(128)(4,1)} %bitcast.66), calls=%async_computation.7 | async-start | bytes 8388608
  694.8 5.7 collective-permute-start.4
  700.8 24.9 %copy-start = (bf16[384,1024]{1,0:T(8,128)(2,1)S(1)}, bf16[384,1024]{1,0:T(8,128)(2,1)}, u32[]{:S(2)}) copy-start(bf16[384,1024]{1,0:T(8,128)(2,1)} %add_convert_fusion.1) | copy-start | bytes 2359300
  700.8 7.3 collective-permute-start.5
  708.1 7.2 collective-permute-start.6
  715.3 7.2 collective-permute-start.7
Sparse Core Ops, SparseCore 0:
  8.9 31.2 all-gather.6
  41.7 149.6 all-gather.10
  192.9 147.7 all-gather.12
  342.2 147.7 all-gather.8
  491.4 147.7 all-gather.14
  659.7 25.7 all-gather.16
